TPU v7x, 32 devices: a whole 2x2x4 slice. The times are simulated.
32 devices in a mesh: kv: 8 (over z, y), tp: 4 (over x, core).
Axes of the slice: x: 2, y: 2, z: 4, core: 2. Of those that a mesh axis runs over, the one named last changes fastest.
Arguments:
- tokens: bfloat16 [3072, 2048], P('kv'), may hold values from -40 to 40
- w_query: bfloat16 [2048, 2048], P(None, 'tp'), may hold values from -0.125 to 0.125
- w_key: bfloat16 [2048, 256], replicated, may hold values from -0.125 to 0.125
- w_value: bfloat16 [2048, 256], replicated, may hold values from -0.125 to 0.125
- w_out: bfloat16 [2048, 2048], P(None, 'tp'), may hold values from -0.125 to 0.125
- chosen: int32 [48, 32], P('kv'), may hold values from -1 to 46, as said below
Outputs:
- mixed: bfloat16 [3072, 2048], P('kv', 'tp')
Inputs may be any that keep to these rules, and one draw needn't show every extreme that they name: `chosen`: row b lists min(b, 32) different blocks below b, block b - 1 among them when b > 0, and -1 in its other entries.
All inputs are finite; a program needn't handle non-finite values.
Results may differ from a plain program's by a relative error of at most 0.015.
The roundings to bfloat16 on the way count: a program that leaves them out, or rounds other values in their place, can miss the bound.
Values may be sent and summed in bfloat16 or wider, within the bound.
A program may use at most 128 MiB of HBM per device.

v0:
```python
import jax
import jax.numpy as jnp
from jax import lax
from jax.sharding import PartitionSpec as P

H = 16
DH = 128
KVH = 2
BLK = 64
NSEL = 32


theta_base = 10000.0


def rotate(values, positions):
    half = values.shape[-1] // 2
    inverse = theta_base ** (-jnp.arange(half, dtype=jnp.float32) / half)
    angles = positions.astype(jnp.float32)[:, None] * inverse[None, :]
    cosine = jnp.cos(angles)[:, None, :]
    sine = jnp.sin(angles)[:, None, :]
    first = values[..., :half]
    second = values[..., half:]
    return jnp.concatenate(
        [first * cosine - second * sine, second * cosine + first * sine], axis=-1
    )


def body(tokens, w_query, w_key, w_value, w_out, chosen):
    rows = tokens.shape[0]
    width = tokens.shape[1]
    tp_count = lax.axis_size("tp")
    tp_index = lax.axis_index("tp")
    kv_index = lax.axis_index("kv")
    split = BLK // tp_count
    local_blocks = rows // BLK
    group = H // KVH
    own_heads = w_query.shape[1] // DH
    slots = NSEL + 1
    positions = kv_index * rows + jnp.arange(rows, dtype=jnp.int32)
    query = jnp.dot(tokens, w_query, preferred_element_type=jnp.float32).reshape(
        rows, own_heads, DH
    )
    query = rotate(query, positions).astype(jnp.bfloat16).reshape(rows, own_heads * DH)
    query_all = lax.all_gather(query, "tp", axis=1, tiled=True)
    offset = tp_index * split
    slab = lax.dynamic_slice_in_dim(tokens.reshape(local_blocks, BLK, width), offset, split, 1)
    slab = slab.reshape(local_blocks * split, width)
    slab_pos = kv_index * rows + jnp.arange(local_blocks, dtype=jnp.int32)[:, None] * BLK + offset
    slab_pos = (slab_pos + jnp.arange(split, dtype=jnp.int32)[None, :]).reshape(-1)
    keys = jnp.dot(slab, w_key, preferred_element_type=jnp.float32).reshape(-1, KVH, DH)
    keys = rotate(keys, slab_pos).astype(jnp.bfloat16).reshape(-1, KVH * DH)
    values = jnp.dot(slab, w_value, preferred_element_type=jnp.float32).astype(jnp.bfloat16)
    first_block = kv_index * local_blocks
    lists = jnp.concatenate(
        [chosen, (first_block + jnp.arange(local_blocks, dtype=jnp.int32))[:, None]], axis=1
    )
    safe = jnp.maximum(lists, 0)
    key_all, value_all = (
        lax.all_gather(keys, "kv", axis=0, tiled=True),
        lax.all_gather(values, "kv", axis=0, tiled=True),
    )
    picked_keys = key_all.reshape(-1, split, KVH * DH)[safe]
    picked_values = value_all.reshape(-1, split, KVH * DH)[safe]
    query_five = query_all.reshape(local_blocks, BLK, KVH, group, DH)
    key_five = picked_keys.reshape(local_blocks, slots, split, KVH, DH)
    scores = jnp.einsum(
        "nqkgd,nsrkd->nkgqsr", query_five, key_five, preferred_element_type=jnp.float32
    ) * DH ** (-0.5)
    query_pos = positions.reshape(local_blocks, BLK)
    key_pos = safe[:, :, None] * BLK + offset + jnp.arange(split, dtype=jnp.int32)[None, None, :]
    allowed = (lists[:, :, None] >= 0)[:, None, :, :] & (
        key_pos[:, None, :, :] <= query_pos[:, :, None, None]
    )
    allowed = allowed[:, None, None]
    scores = jnp.where(allowed, scores, -jnp.inf)
    local_top = jnp.max(scores, axis=(4, 5))
    top = lax.pmax(local_top, "tp")
    weights = jnp.where(allowed, jnp.exp(scores - top[..., None, None]), 0.0)
    total_local = jnp.sum(weights, axis=(4, 5))
    probs = weights.astype(jnp.bfloat16)
    value_five = picked_values.reshape(local_blocks, slots, split, KVH, DH)
    part = jnp.einsum("nkgqsr,nsrkd->nqkgd", probs, value_five, preferred_element_type=jnp.float32)
    part = part.astype(jnp.bfloat16).reshape(1, rows, H * DH)
    moved = lax.all_to_all(part, "tp", split_axis=2, concat_axis=0, tiled=True)
    summed = jnp.sum(moved.astype(jnp.float32), axis=0).reshape(rows, own_heads, DH)
    totals = jnp.transpose(total_local, (0, 3, 1, 2)).reshape(rows, H)
    whole_totals = lax.psum(totals, "tp")
    mine = lax.dynamic_slice_in_dim(whole_totals, tp_index * own_heads, own_heads, 1)
    attention = (summed / mine[:, :, None]).astype(jnp.bfloat16).reshape(rows, own_heads * DH)
    result = jnp.dot(
        lax.all_gather(attention, "tp", axis=1, tiled=True),
        w_out,
        preferred_element_type=jnp.float32,
    )
    return result.astype(jnp.bfloat16)


def solution(mesh):
    placed = (P("kv", None), P(None, "tp"), P(), P(), P(None, "tp"), P("kv", None))
    return jax.shard_map(body, mesh=mesh, in_specs=placed, out_specs=P("kv", "tp"), check_vma=False)
```

profile of v0, /device:TPU:25, one launch (start us, length us, event | category | flops | bytes accessed | tf_op | source)
XLA Modules:
  0.0 264.1 jit_solution(6446708634427179163)
XLA Ops:
  6.6 1.6 copy-done
  8.1 2.4 fusion.21
  10.5 0.3 reshape.259
  10.8 0.8 multiply_cosine_fusion
  11.5 0.6 subtract_convert_fusion
  12.2 0.5 pad_maximum_fusion
  12.8 0.8 copy.77
  13.6 0.6 copy.46
  14.3 0.1 add_convert_fusion.2
  14.3 0.1 convert_element_type.56
  14.4 0.3 multiply_cosine_fusion.1
  14.7 0.1 add_maximum_fusion
  14.8 0.1 reshape.266
  14.9 1.0 constant_dynamic-slice_fusion.1
  15.9 0.5 fusion.20
  16.4 0.1 subtract_convert_fusion.1
  16.5 0.1 copy_bitcast_fusion.1
  16.6 22.3 %all_gather.13 = bf16[768,256]{1,0:T(8,128)(2,1)S(1)} all-gather(bf16[96,256]{1,0:T(8,128)(2,1)S(1)} %copy_bitcast_fusion.1), channel_id=1, replica_groups=mesh['kv'=8,'tp'=4] {'kv'}, dimensions={0}, use_global_device_ids=true | all-gather | bytes 442368 | tf_op jit(solution)/shard_map/all_gather | solution.py:60
  38.9 0.8 gather_fusion.1
  39.7 1.9 reshape.258
  41.6 0.3 convolution_convert_fusion.1
  41.9 25.2 %all_gather.12 = bf16[768,256]{1,0:T(8,128)(2,1)S(1)} all-gather(bf16[96,256]{1,0:T(8,128)(2,1)S(1)} %convolution_convert_fusion.1), channel_id=1, replica_groups=mesh['kv'=8,'tp'=4] {'kv'}, dimensions={0}, use_global_device_ids=true | all-gather | bytes 442368 | tf_op jit(solution)/shard_map/all_gather | solution.py:61
  67.2 0.8 gather_fusion
  68.0 1.9 reshape.256
  69.9 0.1 broadcast_compare_fusion
  70.0 0.1 multiply_add_fusion
  70.1 0.1 iota_add_fusion
  70.2 0.9 compare_and_fusion
  71.1 1.9 copy.54
  73.0 11.1 %fusion = (f32[6,2,8,64]{3,2,1,0:T(8,128)S(1)}, f32[6,2,33,16,64,8]{4,3,5,2,1,0:T(8,128)}) fusion(pred[6,64,33,16]{1,3,2,0:T(8,128)(4,1)S(1)} %compare_and_fusion, bf16[6,64,2,8,128,1]{4,3,2,1,0,5:T(8,128)(2,1)S(1)} %bitcast.72, bf16[6,33,16,2,128,1]{4,3,2,1,0,5:T(2,128)(2,1)S(1)} %bitcast.71), kind=kOutput, calls=%fused_computation.4 | convolution fusion | flops 840198144 | bytes 16398336 | tf_op jit(solution)/shard_map/nqkgd,nsrkd->nkgqsr/dot_general | solution.py:67
  84.1 22.6 %pmax.7 = f32[6,2,8,64]{3,2,1,0:T(8,128)S(1)} all-reduce(f32[6,2,8,64]{3,2,1,0:T(8,128)S(1)} %get-tuple-element.15), channel_id=1, replica_groups=mesh['kv'=8,'tp'=4] {'tp'}, use_global_device_ids=true, to_apply=%region_1.2 | all-reduce | flops 6144 | bytes 49152 | tf_op jit(solution)/shard_map/pmax | solution.py:78
  106.7 16.9 %fusion.1 = (f32[6,2,8,64]{3,2,1,0:T(8,128)S(1)}, bf16[6,2,8,64,33,16]{3,5,2,4,1,0:T(8,128)(2,1)}) fusion(f32[6,2,33,16,64,8]{4,3,5,2,1,0:T(8,128)} %get-tuple-element.16, f32[6,2,8,64]{3,2,1,0:T(8,128)S(1)} %pmax.7, pred[6,64,33,16]{1,3,2,0:T(8,128)(4,1)S(1)} %compare_and_fusion), kind=kLoop, calls=%fused_computation.5 | loop fusion | flops 19458048 | bytes 19716096 | tf_op jit(solution)/shard_map/reduce_sum | solution.py:80
  123.6 17.0 %fusion.13 = bf16[6,64,2,8,128]{4,1,3,2,0:T(8,128)(2,1)} fusion(bf16[6,2,8,64,33,16]{3,5,2,4,1,0:T(8,128)(2,1)} %get-tuple-element.6, bf16[6,33,16,2,128,1]{4,3,2,1,0,5:T(2,128)(2,1)S(1)} %bitcast.76), kind=kOutput, calls=%fused_computation.15 | convolution fusion | flops 831258624 | bytes 9682944 | tf_op jit(solution)/shard_map/nkgqsr,nsrkd->nqkgd/dot_general | solution.py:83
  140.7 2.6 %copy.37 = bf16[6,64,2,8,128]{4,3,2,1,0:T(8,128)(2,1)S(1)} copy(bf16[6,64,2,8,128]{4,1,3,2,0:T(8,128)(2,1)} %fusion.13) | data formatting | bytes 3145728 | tf_op jit(solution)/shard_map/convert_element_type | solution.py:84
  143.3 2.1 reshape.261
  145.4 8.5 %copy.38 = bf16[1,384,2048]{1,0,2:T(2,128)(2,1)} copy(bf16[1,384,2048]{2,1,0:T(8,128)(2,1)} %reshape.261) | data formatting | bytes 3145728 | tf_op jit(solution)/shard_map/reshape | solution.py:84
  153.9 0.5 broadcast.190
  154.4 34.3 %reduce.3 = bf16[2048,384]{1,0:T(8,128)(2,1)S(1)} reduce(bf16[2048,1,384]{2,1,0:T(2,128)(2,1)} %bitcast.66, bf16[]{:T(256)} %broadcast.190), dimensions={1}, to_apply=%bitcast.54.reduce_sub_computation | reduce | bytes 3145730
  188.7 1.9 reshape.289
  190.6 3.9 %all-to-all-start = ((bf16[4,2,98304]{2,1,0:T(2,128)(2,1)}), bf16[4,2,98304]{2,1,0:T(2,128)(2,1)S(1)}, u32[]{:S(2)}, u32[]{:S(2)}) async-start(bf16[4,2,98304]{2,1,0:T(2,128)(2,1)} %reshape.289), calls=%async_computation | async-start | bytes 3145728 | tf_op jit(solution)/shard_map/all_to_all | solution.py:85
  194.5 0.1 reshape.262
  194.6 25.5 %psum.7 = f32[384,16]{0,1:T(8,128)S(1)} all-reduce(f32[384,16]{0,1:T(8,128)S(1)} %reshape.262), channel_id=1, replica_groups=mesh['kv'=8,'tp'=4] {'tp'}, use_global_device_ids=true, to_apply=%region_4.5 | all-reduce | flops 6144 | bytes 49152 | tf_op jit(solution)/shard_map/psum | solution.py:88
  220.1 2.8 %reshape.290 = bf16[2048,1,384]{2,1,0:T(2,128)(2,1)} reshape(bf16[4,2,98304]{2,1,0:T(2,128)(2,1)S(1)} %all-to-all-done) | data formatting | bytes 3145728
  222.9 3.8 %copy.51 = f32[1,384,2048]{1,2,0:T(8,128)} copy(bf16[1,384,2048]{1,0,2:T(2,128)(2,1)} %bitcast.68) | data formatting | bytes 4718592
  226.6 2.1 reduce_sum.18
  228.8 0.8 fusion.18
  229.6 23.8 %all-gather.5.cloned.1.call-done = bf16[384,2048]{0,1:T(8,128)(2,1)} async-done(((bf16[384,512]{0,1:T(8,128)(2,1)}), bf16[384,2048]{0,1:T(8,128)(2,1)}) %all-gather.5.cloned.1.call-update) | async-done | bytes 1572880 | tf_op jit(solution)/shard_map/all_gather | solution.py:92
  253.4 3.8 %convolution_convert_fusion = bf16[384,512]{1,0:T(8,128)(2,1)} fusion(bf16[384,2048]{0,1:T(8,128)(2,1)} %all-gather.5.cloned.1.call-done, bf16[2048,512]{1,0:T(8,128)(2,1)} %param.10), kind=kOutput, calls=%fused_computation.16 | convolution fusion | flops 805502976 | bytes 4063232 | tf_op jit(solution)/shard_map/dot_general | solution.py:91
  (28 shorter events, 0.2 us)
Async XLA Ops:
  6.5 1.6 copy-start
  6.5 64.6 %all-gather.3.cloned.1.call-start = ((), (), s32[]{:S(2)}) async-start(), calls=%async_computation.1 | async-start | bytes 1966080 | tf_op jit(solution)/shard_map/all_gather | solution.py:45
  12.2 1.4 copy-start.4
  12.7 1.9 copy-start.6
  39.7 1.9 copy-start.5
  71.1 2.0 copy-start.2
  106.7 17.0 %copy-start.3 = (bf16[6,33,16,2,128]{4,3,2,1,0:T(2,128)(2,1)S(1)}, bf16[6,33,16,2,128]{4,3,2,1,0:T(2,128)(2,1)}, u32[]{:S(2)}) copy-start(bf16[6,33,16,2,128]{4,3,2,1,0:T(2,128)(2,1)} %reshape.256) | copy-start | bytes 4866052
  190.6 29.5 %all-to-all-start = ((bf16[4,2,98304]{2,1,0:T(2,128)(2,1)}), bf16[4,2,98304]{2,1,0:T(2,128)(2,1)S(1)}, u32[]{:S(2)}, u32[]{:S(2)}) async-start(bf16[4,2,98304]{2,1,0:T(2,128)(2,1)} %reshape.289), calls=%async_computation | async-start | bytes 3145728 | tf_op jit(solution)/shard_map/all_to_all | solution.py:85
  194.5 58.9 %all-gather.5.cloned.1.call-start = ((), (), s32[]{:S(2)}) async-start(), calls=%async_computation.2 | async-start | bytes 1966080 | tf_op jit(solution)/shard_map/all_gather | solution.py:92
  229.6 27.6 %copy-start.1 = (bf16[2048,512]{1,0:T(8,128)(2,1)S(1)}, bf16[2048,512]{1,0:T(8,128)(2,1)}, u32[]{:S(2)}) copy-start(bf16[2048,512]{1,0:T(8,128)(2,1)} %param.7) | copy-start | bytes 6291460
Sparse Core Ops, SparseCore 0:
  13.7 20.9 all-gather.2
  229.7 23.6 all-gather.4
where the time goes:
time: 266 us; the launch traced here: 264 us
  blocking collectives  95.6 us (36%)
  other arithmetic  57.9 us (22%)
  matrix products  35.1 us (13%)
  local copies, waits for them, and re-layouts  34.1 us (13%)
  waiting for transfers between devices  23.8 us (9%)
  between operations  13.7 us (5%)
  starting transfers between devices  3.91 us (1%)
    unnamed x1, other arithmetic  34.3 us
    psum x1, blocking collectives, body(): whole_totals = lax.psum(totals, 'tp')  25.5 us
    all_gather x1, blocking collectives, body(): lax.all_gather(values, 'kv', axis=0, tiled=True)  25.2 us
    all_gather x1, waiting for transfers between devices, body(): lax.all_gather(attention, 'tp', axis=1, tiled=True)  23.8 us
    pmax x1, blocking collectives, body(): top = lax.pmax(local_top, 'tp')  22.6 us
    all_gather x1, blocking collectives, body(): lax.all_gather(keys, 'kv', axis=0, tiled=True)  22.3 us
    dot_general x1, matrix products, body(): jnp.einsum('nkgqsr,nsrkd->nqkgd', probs, value_five, preferred_element_ty...  17 us
    reduce_sum x1, other arithmetic, body(): total_local = jnp.sum(weights, axis=(4, 5))  16.9 us
  transfers between devices with their start and end apart: 3, of which 1 were waited for; matrix products, arithmetic and copies ran while one was open for 4% of the time, Pallas kernels for 0%

commit v1 on v0

v1 whole, which is shorter than its diff:
```python
import functools
import math

import jax
import jax.numpy as jnp
from jax import lax
from jax.experimental import pallas as pl
from jax.experimental.pallas import tpu as pltpu
from jax.sharding import PartitionSpec as P

H = 16
DH = 128
KVH = 2
BLK = 64
NSEL = 32
GROUPS = 4

theta_base = 10000.0
MESH = pl.DeviceIdType.MESH


def rotary_tables(rows, kv_index):
    half = DH // 2
    positions = kv_index * rows + jnp.arange(rows, dtype=jnp.int32)
    inverse = theta_base ** (-jnp.arange(half, dtype=jnp.float32) / half)
    angles = positions.astype(jnp.float32)[:, None] * inverse[None, :]
    cosine = jnp.cos(angles)
    sine = jnp.sin(angles)
    return jnp.concatenate([cosine, cosine], axis=1), jnp.concatenate([-sine, sine], axis=1)


def kernel(
    kv_n, tp_n,
    tokens_hbm, wq_hbm, wk_hbm, wv_hbm, wo_hbm, cos_ref, sin_ref, chosen_ref,
    out_ref,
    tokens, wq, wkv, wo, kv_all, q_all, s_ref, own_ref, vexp, att,
    in_sem, kv_send, kv_recv, att_send, att_fwd, att_recv,
):
    rows, width = tokens.shape
    own = wq.shape[1] // DH
    blocks = rows // BLK
    split = BLK // GROUPS
    out_cols = wo.shape[1]
    qrows = own * BLK
    j = lax.axis_index("kv")
    t = lax.axis_index("tp")
    core = lax.rem(t, 2)
    chip = lax.div(t, 2)
    partner = t + 1 - 2 * core
    y = lax.rem(j, 2)
    z = lax.div(j, 2)
    other = j + 1 - 2 * y
    has_next = j + 2 < kv_n
    has_prev = j >= 2
    head = lax.div(t * own, H // KVH)
    chips = tp_n // 2

    column = pl.ds(pl.multiple_of(head * DH, DH), DH)
    in_copies = [
        pltpu.make_async_copy(tokens_hbm, tokens, in_sem.at[0]),
        pltpu.make_async_copy(wk_hbm.at[:, column], wkv.at[:, pl.ds(0, DH)], in_sem.at[1]),
        pltpu.make_async_copy(wv_hbm.at[:, column], wkv.at[:, pl.ds(DH, DH)], in_sem.at[2]),
        pltpu.make_async_copy(wq_hbm, wq, in_sem.at[3]),
        pltpu.make_async_copy(wo_hbm, wo, in_sem.at[4]),
    ]
    for copy in in_copies:
        copy.start()

    barrier = pltpu.get_barrier_semaphore()

    def greet(kv_at, tp_at):
        pl.semaphore_signal(barrier, inc=1, device_id=(kv_at, tp_at), device_id_type=MESH)

    greet(other, t)
    greet(j, partner)
    for step in range(1, chips):
        greet(j, lax.rem(chip + step, chips) * 2 + core)

    @pl.when(has_next)
    def _():
        greet(j + 2, t)

    @pl.when(has_prev)
    def _():
        greet(j - 2, t)

    expected = 2 + chips - 1 + has_next.astype(jnp.int32) + has_prev.astype(jnp.int32)

    def chunk_copy(c, kind, kv_at):
        where = kv_all.at[core, pl.ds(c * blocks, blocks)]
        return pltpu.make_async_remote_copy(
            src_ref=where, dst_ref=where, send_sem=kv_send.at[kind, c], recv_sem=kv_recv.at[0, c],
            device_id=(kv_at, t), device_id_type=MESH,
        )

    def swap_copy(c):
        where = kv_all.at[core, pl.ds(c * blocks, blocks)]
        return pltpu.make_async_remote_copy(
            src_ref=where, dst_ref=where, send_sem=kv_send.at[2, c], recv_sem=kv_recv.at[1, c],
            device_id=(j, partner), device_id_type=MESH,
        )

    for copy in in_copies[:3]:
        copy.wait()
    tall = rows // 2 if blocks % 2 == 0 else rows
    tall_blocks = tall // BLK

    def project_kv(i, _):
        at = pl.multiple_of(i * tall, BLK)
        kv = jnp.dot(tokens[pl.ds(at, tall), :], wkv[...], preferred_element_type=jnp.float32)
        k = kv[:, :DH]
        k = k * cos_ref[pl.ds(at, tall), :] + pltpu.roll(k, DH // 2, 1) * sin_ref[pl.ds(at, tall), :]
        dst = pl.ds(j * blocks + i * tall_blocks, tall_blocks)
        shape = (tall_blocks, GROUPS, split, DH)
        kv_all[0, dst] = k.astype(jnp.bfloat16).reshape(shape)
        kv_all[1, dst] = kv[:, DH:].astype(jnp.bfloat16).reshape(shape)
        return 0

    lax.fori_loop(0, rows // tall, project_kv, 0)

    pl.semaphore_wait(barrier, expected)

    @pl.when(has_next)
    def _():
        chunk_copy(j, 0, j + 2).start()

    @pl.when(y == 0)
    def _():
        chunk_copy(j, 1, other).start()

    in_copies[3].wait()

    def project_q(i, _):
        at = pl.multiple_of(i * tall, BLK)
        x = tokens[pl.ds(at, tall), :]
        cosine = cos_ref[pl.ds(at, tall), :]
        sine = sin_ref[pl.ds(at, tall), :]
        for pair in range(own // 2):
            q2 = jnp.dot(x, wq[:, pair * 2 * DH:(pair + 1) * 2 * DH], preferred_element_type=jnp.float32)
            for k in range(2):
                q = q2[:, k * DH:(k + 1) * DH]
                q = (q * cosine + pltpu.roll(q, DH // 2, 1) * sine).astype(jnp.bfloat16)
                h = pair * 2 + k
                for n in range(tall_blocks):
                    q_all[i * tall_blocks + n, h * BLK:(h + 1) * BLK, :] = q[n * BLK:(n + 1) * BLK, :]
        return 0

    lax.fori_loop(0, rows // tall, project_q, 0)

    def relay_y(m):
        c = other - 2 * m
        chunk_copy(c, 1, other).wait_recv()
        swap_copy(c).start()

    @pl.when(y == 1)
    def _():
        relay_y(0)

    def relay(m, _):
        c = j - 2 * m
        chunk_copy(c, 0, other).wait_recv()

        @pl.when(has_next)
        def _():
            chunk_copy(c, 0, j + 2).start()

        chunk_copy(c, 1, other).start()
        swap_copy(c).start()
        relay_y(m)
        return 0

    lax.fori_loop(1, z + 1, relay, 0)

    def take(c, _):
        there = kv_all.at[1 - core, pl.ds(c * blocks, blocks)]
        pltpu.make_async_remote_copy(
            src_ref=there, dst_ref=there, send_sem=kv_send.at[2, c], recv_sem=kv_recv.at[1, c],
            device_id=(j, partner), device_id_type=MESH,
        ).wait_recv()
        return 0

    lax.fori_loop(0, j, take, 0)

    factor = DH ** -0.5 * math.log2(math.e)
    wide = NSEL * split

    def att_copy(source, n, sem, tp_at):
        where = att.at[source, pl.ds(pl.multiple_of(n * BLK, BLK), BLK)]
        return pltpu.make_async_remote_copy(
            src_ref=where, dst_ref=where, send_sem=sem, recv_sem=att_recv.at[source, n],
            device_id=(j, tp_at), device_id_type=MESH,
        )

    def peer(step):
        return lax.rem(chip + step, chips) * 2 + core

    def send_att(n):
        att_copy(t, n, att_send.at[0, n], partner).start()
        for step in range(1, chips):
            att_copy(t, n, att_send.at[step, n], peer(step)).start()

    def forward_att(n):
        for step in range(1, chips):
            source = peer(step)
            att_copy(source, n, att_fwd.at[step, n], partner).wait_recv()
            att_copy(source, n, att_fwd.at[step, n], partner).start()

    def attend(n, _):
        b = j * blocks + n
        valid = jnp.minimum(b, NSEL)
        index = [chosen_ref[n, s] for s in range(NSEL)]
        q = q_all[n]
        nt = (((1,), (1,)), ((), ()))
        so = lax.dot_general(q, kv_all[0, b].reshape(BLK, DH), nt, preferred_element_type=jnp.float32)
        qpos = lax.rem(lax.broadcasted_iota(jnp.int32, (qrows, BLK), 0), BLK)
        kpos = lax.broadcasted_iota(jnp.int32, (qrows, BLK), 1)
        so = jnp.where(kpos <= qpos, so, -jnp.inf)
        own_ref[...] = so
        slot = lax.div(lax.broadcasted_iota(jnp.int32, (1, wide), 1), split)
        bias = jnp.where(slot < valid, 0.0, -jnp.inf).astype(jnp.float32)
        running = None
        for g in range(GROUPS):
            k = jnp.concatenate(
                [kv_all[0, i, g] for i in index], axis=0
            )
            s = lax.dot_general(q, k, nt, preferred_element_type=jnp.float32) + bias
            s_ref[g] = s
            for piece in range(wide // DH):
                tile = s[:, piece * DH:(piece + 1) * DH]
                running = tile if running is None else jnp.maximum(running, tile)
        top = jnp.maximum(
            jnp.max(running, axis=1, keepdims=True), jnp.max(so, axis=1, keepdims=True)
        )
        po = jnp.exp2((own_ref[...] - top) * factor)
        total = jnp.sum(po, axis=1, keepdims=True)
        vo = kv_all[1, b].reshape(BLK, DH)
        for g in range(GROUPS):
            vexp[g * split:(g + 1) * split, g * DH:(g + 1) * DH] = vo[g * split:(g + 1) * split, :]
        from_own = jnp.dot(po.astype(jnp.bfloat16), vexp[...], preferred_element_type=jnp.float32)
        sums = None
        summed = None
        for g in range(GROUPS):
            v = jnp.concatenate(
                [kv_all[1, i, g] for i in index], axis=0
            )
            p = jnp.exp2((s_ref[g] - top) * factor)
            for piece in range(wide // DH):
                tile = p[:, piece * DH:(piece + 1) * DH]
                sums = tile if sums is None else sums + tile
            part = jnp.dot(p.astype(jnp.bfloat16), v, preferred_element_type=jnp.float32)
            part = (part + from_own[:, g * DH:(g + 1) * DH]).astype(jnp.bfloat16).astype(jnp.float32)
            summed = part if summed is None else summed + part
        total = total + jnp.sum(sums, axis=1, keepdims=True)
        a = (summed / total).astype(jnp.bfloat16)
        for h in range(own):
            att[t, pl.ds(pl.multiple_of(n * BLK, BLK), BLK), h * DH:(h + 1) * DH] = a[h * BLK:(h + 1) * BLK, :]
        send_att(n)

        @pl.when(n >= 1)
        def _():
            forward_att(n - 1)

        return 0

    vexp[...] = jnp.zeros_like(vexp)
    lax.fori_loop(0, blocks, attend, 0)
    forward_att(blocks - 1)

    in_copies[4].wait()

    def arrive(n, _):
        for c in range(chips):
            source = c * 2 + 1 - core
            att_copy(source, n, att_fwd.at[0, n], partner).wait_recv()
        return 0

    lax.fori_loop(0, blocks, arrive, 0)

    def project_out(i, _):
        at = pl.multiple_of(i * tall, BLK)
        step = min(out_cols, 256)
        for part in range(out_cols // step):
            acc = None
            for source in range(tp_n):
                term = jnp.dot(
                    att[source, pl.ds(at, tall), :],
                    wo[source * own * DH:(source + 1) * own * DH, part * step:(part + 1) * step],
                    preferred_element_type=jnp.float32,
                )
                acc = term if acc is None else acc + term
            out_ref[pl.ds(at, tall), part * step:(part + 1) * step] = acc.astype(jnp.bfloat16)
        return 0

    lax.fori_loop(0, rows // tall, project_out, 0)

    @pl.when(has_next)
    def _():
        chunk_copy(j, 0, j + 2).wait_send()

    @pl.when(y == 0)
    def _():
        chunk_copy(j, 1, other).wait_send()

    @pl.when(y == 1)
    def _():
        swap_copy(other).wait_send()

    def drain(m, _):
        c = j - 2 * m

        @pl.when(has_next)
        def _():
            chunk_copy(c, 0, j + 2).wait_send()

        chunk_copy(c, 1, other).wait_send()
        swap_copy(c).wait_send()
        swap_copy(other - 2 * m).wait_send()
        return 0

    lax.fori_loop(1, z + 1, drain, 0)

    def drain_att(n, _):
        att_copy(t, n, att_send.at[0, n], partner).wait_send()
        for step in range(1, chips):
            att_copy(t, n, att_send.at[step, n], peer(step)).wait_send()
            att_copy(peer(step), n, att_fwd.at[step, n], partner).wait_send()
        return 0

    lax.fori_loop(0, blocks, drain_att, 0)


def body(kv_n, tp_n, tokens, w_query, w_key, w_value, w_out, chosen):
    rows, width = tokens.shape
    own_cols = w_query.shape[1]
    own = own_cols // DH
    blocks = rows // BLK
    cosine, sine = rotary_tables(rows, lax.axis_index("kv"))
    number = (lax.axis_index("kv") * blocks + jnp.arange(blocks, dtype=jnp.int32))[:, None]
    slot = jnp.arange(NSEL, dtype=jnp.int32)[None, :]
    listed = jnp.where(number <= NSEL, slot, chosen)
    listed = jnp.where(slot < number, listed, 0)
    anywhere = pl.BlockSpec(memory_space=pl.ANY)
    vmem = pl.BlockSpec(memory_space=pltpu.VMEM)
    bf16 = jnp.bfloat16
    chips = tp_n // 2
    return pl.pallas_call(
        functools.partial(kernel, kv_n, tp_n),
        name="sparse_attention",
        out_shape=jax.ShapeDtypeStruct((rows, w_out.shape[1]), bf16),
        in_specs=[anywhere] * 5 + [vmem] * 2 + [pl.BlockSpec(memory_space=pltpu.SMEM)],
        out_specs=vmem,
        scratch_shapes=[
            pltpu.VMEM((rows, width), bf16),
            pltpu.VMEM(w_query.shape, bf16),
            pltpu.VMEM((width, 2 * DH), bf16),
            pltpu.VMEM(w_out.shape, bf16),
            pltpu.VMEM((2, kv_n * blocks, GROUPS, BLK // GROUPS, DH), bf16),
            pltpu.VMEM((blocks, own * BLK, DH), bf16),
            pltpu.VMEM((GROUPS, own * BLK, NSEL * BLK // GROUPS), jnp.float32),
            pltpu.VMEM((own * BLK, BLK), jnp.float32),
            pltpu.VMEM((BLK, GROUPS * DH), bf16),
            pltpu.VMEM((tp_n, rows, own_cols), bf16),
            pltpu.SemaphoreType.DMA((5,)),
            pltpu.SemaphoreType.DMA((3, kv_n)),
            pltpu.SemaphoreType.DMA((2, kv_n)),
            pltpu.SemaphoreType.DMA((chips, blocks)),
            pltpu.SemaphoreType.DMA((chips, blocks)),
            pltpu.SemaphoreType.DMA((tp_n, blocks)),
        ],
        compiler_params=pltpu.CompilerParams(
            collective_id=0, has_side_effects=True, vmem_limit_bytes=56 * 1024 * 1024
        ),
    )(tokens, w_query, w_key, w_value, w_out, cosine, sine, listed)


def solution(mesh):
    placed = (P("kv", None), P(None, "tp"), P(), P(), P(None, "tp"), P("kv", None))
    return jax.shard_map(
        functools.partial(body, mesh.shape["kv"], mesh.shape["tp"]),
        mesh=mesh, in_specs=placed, out_specs=P("kv", "tp"), check_vma=False,
    )
```

time: 266 us -> 44.9 us (0.17)
  blocking collectives: 95.6 us -> 0 us
  other arithmetic: 57.9 us -> 3.05 us
  Pallas kernels: 0 us -> 39.9 us
  matrix products: 35.1 us -> 0 us
  local copies, waits for them, and re-layouts: 34.1 us -> 1.77 us
  waiting for transfers between devices: 23.8 us -> 0 us
  between operations: 13.7 us -> 0.02 us
  starting transfers between devices: 3.91 us -> 0 us
    all_gather x2 -> x0, blocking collectives: 47.6 us -> none  [the longest x1 25.2 us: body(): lax.all_gather(values, 'kv', axis=0, tiled=True)]
    pallas_call x0 -> x1, Pallas kernels: none -> 39.9 us  [body(): pl.pallas_call(functools.partial(kernel, kv_n, tp_n), name='sparse_attent...]
    dot_general x6 -> x0, matrix products: 35.1 us -> none  [the longest x1 17 us: body(): jnp.einsum('nkgqsr,nsrkd->nqkgd', probs, value_five, preferred_element_ty...]
    unnamed x1 -> x0, other arithmetic: 34.3 us -> none
    psum x1 -> x0, blocking collectives: 25.5 us -> none  [body(): whole_totals = lax.psum(totals, 'tp')]
    all_gather x2 -> x0, waiting for transfers between devices: 23.8 us -> none  [the longest x1 23.8 us: body(): lax.all_gather(attention, 'tp', axis=1, tiled=True)]
    pmax x1 -> x0, blocking collectives: 22.6 us -> none  [body(): top = lax.pmax(local_top, 'tp')]
    reduce_sum x2 -> x0, other arithmetic: 19.1 us -> none  [the longest x1 16.9 us: body(): total_local = jnp.sum(weights, axis=(4, 5))]
  transfers between devices with their start and end apart: 3 -> 0, of which waited for: 1 -> 0; matrix products, arithmetic and copies ran while one was open for 4% -> 0% of each run, Pallas kernels for 0% -> 0%
where the time goes in v1:
time: 44.9 us; the launch traced here: 44.7 us
  Pallas kernels  39.9 us (89%)
  other arithmetic  3.05 us (7%)
  local copies, waits for them, and re-layouts  1.77 us (4%)
    pallas_call x1, Pallas kernels, body(): pl.pallas_call(functools.partial(kernel, kv_n, tp_n), name='sparse_attent...  39.9 us
    unnamed x1, local copies, waits for them, and re-layouts  1.77 us
    select_n x1, other arithmetic, body(): listed = jnp.where(slot < number, listed, 0)  1.34 us
    concatenate x1, other arithmetic, rotary_tables(): jnp.concatenate([cosine, cosine], axis=1)  0.92 us

profile of v1, /device:TPU:25, one launch (start us, length us, event | category | flops | bytes accessed | tf_op | source)
XLA Modules:
  0.0 44.7 jit_solution(2324258622611770308)
XLA Ops:
  0.0 0.8 %fusion = (f32[384,64]{1,0:T(8,128)S(1)}, f32[384,64]{1,0:T(8,128)S(1)}, f32[384,64]{1,0:T(8,128)S(1)}) fusion(f32[64]{0:T(128)S(1)} %multiply_power_fusion, f32[384]{0:T(512)S(1)} %add_convert_fusion), kind=kLoop, calls=%fused_computation.4 | loop fusion | flops 49152 | bytes 296704 | tf_op jit(solution)/shard_map/neg | solution.py:29
  0.8 0.9 %pad_maximum_fusion = (f32[384,128]{1,0:T(8,128)}, f32[384,128]{1,0:T(8,128)}) fusion(f32[384,64]{1,0:T(8,128)S(1)} %get-tuple-element.7, f32[384,64]{1,0:T(8,128)S(1)} %get-tuple-element.6, f32[384,64]{1,0:T(8,128)S(1)} %get-tuple-element.5), kind=kLoop, calls=%fused_computation.2 | loop fusion | flops 98304 | bytes 688128 | tf_op jit(solution)/shard_map/concatenate | solution.py:29
  1.7 1.3 %select_select_fusion.chosen_ref = s32[6,32]{1,0:T(8,128)} fusion(s32[6,32]{1,0:T(8,128)} %param.11, s32[6]{0:T(128)S(1)} %iota_add_fusion, pred[6]{0:T(512)(128)(4,1)S(1)} %broadcast_compare_fusion), kind=kLoop, calls=%fused_computation.5 | loop fusion | flops 576 | bytes 1566 | tf_op jit(solution)/shard_map/jit(_where)/select_n | solution.py:341
  3.1 39.9 %sparse_attention.1 = bf16[384,512]{1,0:T(8,128)(2,1)} custom-call(bf16[384,2048]{1,0:T(8,128)(2,1)} %tokens_hbm.1, bf16[2048,512]{1,0:T(8,128)(2,1)} %wq_hbm.1, bf16[2048,256]{1,0:T(8,128)(2,1)} %wk_hbm.1, bf16[2048,256]{1,0:T(8,128)(2,1)} %wv_hbm.1, bf16[2048,512]{1,0:T(8,128)(2,1)} %wo_hbm.1, f32[384,128]{1,0:T(8,128)} %get-tuple-element.8.cos_ref, ...), custom_call_target="tpu_custom_call" | custom-call | tf_op jit(solution)/shard_map/sparse_attention/pallas_call | solution.py:346
  42.9 1.8 %copy.8 = bf16[384,512]{1,0:T(8,128)(2,1)} copy(bf16[384,512]{1,0:T(8,128)(2,1)} %sparse_attention.1) | data formatting | bytes 786432
  (4 shorter events, 0.0 us)

commit v2 on v1

v2 whole, which is shorter than its diff:
```python
import functools
import math

import jax
import jax.numpy as jnp
from jax import lax
from jax.experimental import pallas as pl
from jax.experimental.pallas import tpu as pltpu
from jax.sharding import PartitionSpec as P

H = 16
DH = 128
KVH = 2
BLK = 64
NSEL = 32
GROUPS = 4

theta_base = 10000.0
MESH = pl.DeviceIdType.MESH


def kernel(
    kv_n, tp_n,
    tokens_hbm, wq_hbm, wk_hbm, wv_hbm, wo_hbm, inverse_ref, chosen_ref,
    out_ref,
    tokens, wq, wkv, wo, cos_ref, sin_ref, k_all, v_all, q_all, s_ref, own_ref, top_ref, vexp, att,
    in_sem, z_send, y_send, swap_send, kv_recv, att_send, att_fwd, att_recv,
):
    rows, width = tokens.shape
    own = wq.shape[1] // DH
    blocks = rows // BLK
    half_blocks = blocks // 2
    tall = rows // 2
    split = BLK // GROUPS
    out_cols = wo.shape[1]
    qrows = own * BLK
    zn = kv_n // 2
    j = lax.axis_index("kv")
    t = lax.axis_index("tp")
    core = lax.rem(t, 2)
    chip = lax.div(t, 2)
    partner = t + 1 - 2 * core
    y = lax.rem(j, 2)
    z = lax.div(j, 2)
    other = j + 1 - 2 * y
    later = zn - 1 - z
    head = lax.div(t * own, H // KVH)
    chips = tp_n // 2

    column = pl.ds(pl.multiple_of(head * DH, DH), DH)
    first_half = pl.ds(pl.multiple_of(core * tall, BLK), tall)
    second_half = pl.ds(pl.multiple_of((1 - core) * tall, BLK), tall)
    in_copies = [
        pltpu.make_async_copy(tokens_hbm.at[first_half], tokens.at[first_half], in_sem.at[0]),
        pltpu.make_async_copy(wk_hbm.at[:, column], wkv.at[:, pl.ds(0, DH)], in_sem.at[1]),
        pltpu.make_async_copy(wv_hbm.at[:, column], wkv.at[:, pl.ds(DH, DH)], in_sem.at[2]),
        pltpu.make_async_copy(tokens_hbm.at[second_half], tokens.at[second_half], in_sem.at[3]),
        pltpu.make_async_copy(wq_hbm, wq, in_sem.at[4]),
        pltpu.make_async_copy(wo_hbm, wo, in_sem.at[5]),
    ]
    for copy in in_copies[:3]:
        copy.start()

    barrier = pltpu.get_barrier_semaphore()

    def greet(kv_at, tp_at):
        pl.semaphore_signal(barrier, inc=1, device_id=(kv_at, tp_at), device_id_type=MESH)

    greet(other, t)
    greet(j, partner)
    for step in range(1, chips):
        greet(j, lax.rem(chip + step, chips) * 2 + core)

    def greet_z(d, _):
        greet(lax.rem(z + d, zn) * 2 + y, t)
        return 0

    lax.fori_loop(1, zn, greet_z, 0)

    def part_of(kind, c, side):
        return (k_all, v_all)[kind].at[pl.ds(c * blocks + side * half_blocks, half_blocks)]

    def z_copy(kind, d):
        where = part_of(kind, j, core)
        return pltpu.make_async_remote_copy(
            src_ref=where, dst_ref=where, send_sem=z_send.at[kind, d], recv_sem=kv_recv.at[kind, 0, j],
            device_id=(j + 2 * d, t), device_id_type=MESH,
        )

    def y_copy(kind, c):
        where = part_of(kind, c, core)
        return pltpu.make_async_remote_copy(
            src_ref=where, dst_ref=where, send_sem=y_send.at[kind, c], recv_sem=kv_recv.at[kind, 0, c],
            device_id=(other, t), device_id_type=MESH,
        )

    def swap_copy(kind, c, side):
        where = part_of(kind, c, side)
        return pltpu.make_async_remote_copy(
            src_ref=where, dst_ref=where, send_sem=swap_send.at[kind, c], recv_sem=kv_recv.at[kind, 1, c],
            device_id=(j, partner), device_id_type=MESH,
        )

    lane = lax.broadcasted_iota(jnp.int32, (BLK, DH), 1)

    def tables(i, _):
        at = pl.ds(pl.multiple_of(i * BLK, BLK), BLK)
        position = (j * rows + i * BLK + lax.broadcasted_iota(jnp.int32, (BLK, DH), 0)).astype(jnp.float32)
        angle = position * inverse_ref[...]
        cos_ref[at, :] = jnp.cos(angle)
        sine = jnp.sin(angle)
        sin_ref[at, :] = jnp.where(lane < DH // 2, -sine, sine)
        return 0

    lax.fori_loop(0, blocks, tables, 0)

    def project_kv(side):
        at = pl.multiple_of(side * tall, BLK)
        kv = jnp.dot(tokens[pl.ds(at, tall), :], wkv[...], preferred_element_type=jnp.float32)
        k = kv[:, :DH]
        k = k * cos_ref[pl.ds(at, tall), :] + pltpu.roll(k, DH // 2, 1) * sin_ref[pl.ds(at, tall), :]
        dst = pl.ds(j * blocks + side * half_blocks, half_blocks)
        shape = (half_blocks, GROUPS, split, DH)
        k_all[dst] = k.astype(jnp.bfloat16).reshape(shape)
        v_all[dst] = kv[:, DH:].astype(jnp.bfloat16).reshape(shape)

    for copy in in_copies[:3]:
        copy.wait()
    for copy in in_copies[3:]:
        copy.start()
    project_kv(core)
    pl.semaphore_wait(barrier, 2 + chips - 1 + zn - 1)
    for kind in range(2):
        @pl.when(y == 0)
        def _():
            y_copy(kind, j).start()

        def send_z(i, _):
            z_copy(kind, later - i).start()
            return 0

        lax.fori_loop(0, later, send_z, 0)
    in_copies[3].wait()
    project_kv(1 - core)

    in_copies[4].wait()

    def project_q(i, _):
        at = pl.multiple_of(i * tall, BLK)
        x = tokens[pl.ds(at, tall), :]
        cosine = cos_ref[pl.ds(at, tall), :]
        sine = sin_ref[pl.ds(at, tall), :]
        for pair in range(own // 2):
            q2 = jnp.dot(x, wq[:, pair * 2 * DH:(pair + 1) * 2 * DH], preferred_element_type=jnp.float32)
            for k in range(2):
                q = q2[:, k * DH:(k + 1) * DH]
                q = (q * cosine + pltpu.roll(q, DH // 2, 1) * sine).astype(jnp.bfloat16)
                h = pair * 2 + k
                for n in range(half_blocks):
                    q_all[i * half_blocks + n, h * BLK:(h + 1) * BLK, :] = q[n * BLK:(n + 1) * BLK, :]
        return 0

    lax.fori_loop(0, 2, project_q, 0)

    def relay_y(kind, m):
        c = other - 2 * m
        y_copy(kind, c).wait_recv()
        swap_copy(kind, c, core).start()

    def relay_first(kind):
        @pl.when(y == 1)
        def _():
            relay_y(kind, 0)

    def relay(kind, m):
        c = j - 2 * m
        y_copy(kind, c).wait_recv()
        y_copy(kind, c).start()
        swap_copy(kind, c, core).start()

        @pl.when(m >= 2)
        def _():
            relay_y(kind, m - 1)

        @pl.when(m == z)
        def _():
            relay_y(kind, m)

    def relay_keys(m, _):
        relay(0, m)
        return 0

    def take(kind):
        def one(c, _):
            swap_copy(kind, c, 1 - core).wait_recv()
            return 0

        lax.fori_loop(0, j, one, 0)

    relay_first(0)
    lax.fori_loop(1, z + 1, relay_keys, 0)
    take(0)

    factor = DH ** -0.5 * math.log2(math.e)
    wide = NSEL * split

    def att_copy(source, n, sem, tp_at):
        where = att.at[source, pl.ds(pl.multiple_of(n * BLK, BLK), BLK)]
        return pltpu.make_async_remote_copy(
            src_ref=where, dst_ref=where, send_sem=sem, recv_sem=att_recv.at[source, n],
            device_id=(j, tp_at), device_id_type=MESH,
        )

    def peer(step):
        return lax.rem(chip + step, chips) * 2 + core

    def send_att(n):
        for step in range(1, chips):
            att_copy(t, n, att_send.at[step, n], peer(step)).start()
        att_copy(t, n, att_send.at[0, n], partner).start()

    def forward_att(n):
        for step in range(1, chips):
            source = peer(step)
            att_copy(source, n, att_fwd.at[step, n], partner).wait_recv()
            att_copy(source, n, att_fwd.at[step, n], partner).start()

    def block_index(n):
        b = j * blocks + n
        many = (b > NSEL).astype(jnp.int32)
        last = jnp.maximum(b - 1, 0)
        return [many * chosen_ref[n, s] + (1 - many) * jnp.minimum(s, last) for s in range(NSEL)]

    def score(n):
        b = j * blocks + n
        index = block_index(n)
        q = q_all[n]
        nt = (((1,), (1,)), ((), ()))
        so = lax.dot_general(q, k_all[b].reshape(BLK, DH), nt, preferred_element_type=jnp.float32)
        qpos = lax.rem(lax.broadcasted_iota(jnp.int32, (qrows, BLK), 0), BLK)
        kpos = lax.broadcasted_iota(jnp.int32, (qrows, BLK), 1)
        so = jnp.where(kpos <= qpos, so, -jnp.inf)
        own_ref[n] = so
        slot = lax.div(lax.broadcasted_iota(jnp.int32, (1, wide), 1), split)
        bias = jnp.where(slot < b, 0.0, -jnp.inf).astype(jnp.float32)
        running = None
        for g in range(GROUPS):
            k = jnp.concatenate([k_all[i, g] for i in index], axis=0)
            s = lax.dot_general(q, k, nt, preferred_element_type=jnp.float32) + bias
            s_ref[n, g] = s
            for piece in range(wide // DH):
                tile = s[:, piece * DH:(piece + 1) * DH]
                running = tile if running is None else jnp.maximum(running, tile)
        top = jnp.maximum(
            jnp.max(running, axis=1, keepdims=True), jnp.max(so, axis=1, keepdims=True)
        )
        top_ref[n] = jnp.broadcast_to(top, (qrows, DH))

    def attend(n):
        b = j * blocks + n
        index = block_index(n)
        top = top_ref[n][:, :1]
        po = jnp.exp2((own_ref[n] - top) * factor)
        total = jnp.sum(po, axis=1, keepdims=True)
        vo = v_all[b].reshape(BLK, DH)
        for g in range(GROUPS):
            vexp[g * split:(g + 1) * split, g * DH:(g + 1) * DH] = vo[g * split:(g + 1) * split, :]
        from_own = jnp.dot(po.astype(jnp.bfloat16), vexp[...], preferred_element_type=jnp.float32)
        sums = None
        summed = None
        for g in range(GROUPS):
            v = jnp.concatenate([v_all[i, g] for i in index], axis=0)
            p = jnp.exp2((s_ref[n, g] - top) * factor)
            for piece in range(wide // DH):
                tile = p[:, piece * DH:(piece + 1) * DH]
                sums = tile if sums is None else sums + tile
            part = jnp.dot(p.astype(jnp.bfloat16), v, preferred_element_type=jnp.float32)
            part = (part + from_own[:, g * DH:(g + 1) * DH]).astype(jnp.bfloat16).astype(jnp.float32)
            summed = part if summed is None else summed + part
        total = total + jnp.sum(sums, axis=1, keepdims=True)
        a = (summed / total).astype(jnp.bfloat16)
        for h in range(own):
            att[t, pl.ds(pl.multiple_of(n * BLK, BLK), BLK), h * DH:(h + 1) * DH] = a[h * BLK:(h + 1) * BLK, :]
        send_att(n)

        @pl.when(n >= 1)
        def _():
            forward_att(n - 1)

    ahead = half_blocks
    per = -(-(zn - 1) // ahead)

    def lead(n, _):
        score(n)

        @pl.when(n == 0)
        def _():
            relay_first(1)

        for k in range(per):
            m = n * per + k + 1

            @pl.when(m <= z)
            def _():
                relay(1, m)

        return 0

    def follow(n, _):
        attend(n)
        score(n + ahead)
        return 0

    def finish(n, _):
        attend(n)
        return 0

    vexp[...] = jnp.zeros_like(vexp)
    lax.fori_loop(0, ahead, lead, 0)
    take(1)
    lax.fori_loop(0, blocks - ahead, follow, 0)
    lax.fori_loop(blocks - ahead, blocks, finish, 0)
    forward_att(blocks - 1)

    in_copies[5].wait()

    def arrive(n, _):
        for c in range(chips):
            source = c * 2 + 1 - core
            att_copy(source, n, att_fwd.at[0, n], partner).wait_recv()
        return 0

    lax.fori_loop(0, blocks, arrive, 0)

    def project_out(i, _):
        at = pl.multiple_of(i * tall, BLK)
        step = min(out_cols, 256)
        for part in range(out_cols // step):
            acc = None
            for source in range(tp_n):
                term = jnp.dot(
                    att[source, pl.ds(at, tall), :],
                    wo[source * own * DH:(source + 1) * own * DH, part * step:(part + 1) * step],
                    preferred_element_type=jnp.float32,
                )
                acc = term if acc is None else acc + term
            out_ref[pl.ds(at, tall), part * step:(part + 1) * step] = acc.astype(jnp.bfloat16)
        return 0

    lax.fori_loop(0, rows // tall, project_out, 0)

    for kind in range(2):
        @pl.when(y == 0)
        def _():
            y_copy(kind, j).wait_send()

        def drain_z(i, _):
            z_copy(kind, i + 1).wait_send()
            return 0

        def drain_y(m, _):
            y_copy(kind, j - 2 * m).wait_send()
            return 0

        def drain_swap(c, _):
            swap_copy(kind, c, core).wait_send()
            return 0

        lax.fori_loop(0, later, drain_z, 0)
        lax.fori_loop(1, z + 1, drain_y, 0)
        lax.fori_loop(0, j, drain_swap, 0)

    def drain_att(n, _):
        att_copy(t, n, att_send.at[0, n], partner).wait_send()
        for step in range(1, chips):
            att_copy(t, n, att_send.at[step, n], peer(step)).wait_send()
            att_copy(peer(step), n, att_fwd.at[step, n], partner).wait_send()
        return 0

    lax.fori_loop(0, blocks, drain_att, 0)


def body(kv_n, tp_n, tokens, w_query, w_key, w_value, w_out, chosen):
    rows, width = tokens.shape
    own_cols = w_query.shape[1]
    own = own_cols // DH
    blocks = rows // BLK
    half = DH // 2
    inverse = theta_base ** (-jnp.arange(half, dtype=jnp.float32) / half)
    inverse = jnp.concatenate([inverse, inverse])[None, :]
    anywhere = pl.BlockSpec(memory_space=pl.ANY)
    vmem = pl.BlockSpec(memory_space=pltpu.VMEM)
    bf16 = jnp.bfloat16
    chips = tp_n // 2
    return pl.pallas_call(
        functools.partial(kernel, kv_n, tp_n),
        name="sparse_attention",
        out_shape=jax.ShapeDtypeStruct((rows, w_out.shape[1]), bf16),
        in_specs=[anywhere] * 5 + [vmem] + [pl.BlockSpec(memory_space=pltpu.SMEM)],
        out_specs=vmem,
        scratch_shapes=[
            pltpu.VMEM((rows, width), bf16),
            pltpu.VMEM(w_query.shape, bf16),
            pltpu.VMEM((width, 2 * DH), bf16),
            pltpu.VMEM(w_out.shape, bf16),
            pltpu.VMEM((rows, DH), jnp.float32),
            pltpu.VMEM((rows, DH), jnp.float32),
            pltpu.VMEM((kv_n * blocks, GROUPS, BLK // GROUPS, DH), bf16),
            pltpu.VMEM((kv_n * blocks, GROUPS, BLK // GROUPS, DH), bf16),
            pltpu.VMEM((blocks, own * BLK, DH), bf16),
            pltpu.VMEM((blocks, GROUPS, own * BLK, NSEL * BLK // GROUPS), jnp.float32),
            pltpu.VMEM((blocks, own * BLK, BLK), jnp.float32),
            pltpu.VMEM((blocks, own * BLK, DH), jnp.float32),
            pltpu.VMEM((BLK, GROUPS * DH), bf16),
            pltpu.VMEM((tp_n, rows, own_cols), bf16),
            pltpu.SemaphoreType.DMA((6,)),
            pltpu.SemaphoreType.DMA((2, kv_n // 2)),
            pltpu.SemaphoreType.DMA((2, kv_n)),
            pltpu.SemaphoreType.DMA((2, kv_n)),
            pltpu.SemaphoreType.DMA((2, 2, kv_n)),
            pltpu.SemaphoreType.DMA((chips, blocks)),
            pltpu.SemaphoreType.DMA((chips, blocks)),
            pltpu.SemaphoreType.DMA((tp_n, blocks)),
        ],
        compiler_params=pltpu.CompilerParams(
            collective_id=0, has_side_effects=True, vmem_limit_bytes=56 * 1024 * 1024
        ),
    )(tokens, w_query, w_key, w_value, w_out, inverse, chosen)


def solution(mesh):
    placed = (P("kv", None), P(None, "tp"), P(), P(), P(None, "tp"), P("kv", None))
    return jax.shard_map(
        functools.partial(body, mesh.shape["kv"], mesh.shape["tp"]),
        mesh=mesh, in_specs=placed, out_specs=P("kv", "tp"), check_vma=False,
    )
```

time: 44.9 us -> 45 us (level)
  other arithmetic: 3.05 us -> 0.6 us
  Pallas kernels: 39.9 us -> 42.1 us
    pallas_call x1, Pallas kernels: 39.9 us -> 42.1 us  [body(): pl.pallas_call(functools.partial(kernel, kv_n, tp_n), name='sparse_attent...]
    select_n x1 -> x0, other arithmetic: 1.34 us -> none  [body(): listed = jnp.where(slot < number, listed, 0)]
    concatenate x1 -> x0, other arithmetic: 0.92 us -> none  [rotary_tables(): jnp.concatenate([cosine, cosine], axis=1)]
    neg x1 -> x0, other arithmetic: 0.77 us -> none  [rotary_tables(): -sine]
    broadcast_in_dim x0 -> x1, other arithmetic: none -> 0.59 us  [body(): inverse = jnp.concatenate([inverse, inverse])[None, :]]
where the time goes in v2:
time: 45 us; the launch traced here: 44.5 us
  Pallas kernels  42.1 us (94%)
  local copies, waits for them, and re-layouts  1.77 us (4%)
  other arithmetic  0.6 us (1%)
    pallas_call x1, Pallas kernels, body(): pl.pallas_call(functools.partial(kernel, kv_n, tp_n), name='sparse_attent...  42.1 us
    unnamed x1, local copies, waits for them, and re-layouts  1.77 us

profile of v2, /device:TPU:25, one launch (start us, length us, event | category | flops | bytes accessed | tf_op | source)
XLA Modules:
  0.0 44.5 jit_solution(9696644626395432969)
XLA Ops:
  0.0 0.6 %maximum_bitcast_fusion.inverse_ref = f32[1,128]{1,0:T(1,128)} fusion(f32[64]{0:T(128)S(1)} %multiply_power_fusion), kind=kLoop, calls=%fused_computation | loop fusion | flops 128 | bytes 768 | tf_op jit(solution)/shard_map/broadcast_in_dim | solution.py:390
  0.6 42.1 %sparse_attention.1 = bf16[384,512]{1,0:T(8,128)(2,1)} custom-call(bf16[384,2048]{1,0:T(8,128)(2,1)} %tokens_hbm.1, bf16[2048,512]{1,0:T(8,128)(2,1)} %wq_hbm.1, bf16[2048,256]{1,0:T(8,128)(2,1)} %wk_hbm.1, bf16[2048,256]{1,0:T(8,128)(2,1)} %wv_hbm.1, bf16[2048,512]{1,0:T(8,128)(2,1)} %wo_hbm.1, f32[1,128]{1,0:T(1,128)} %maximum_bitcast_fusion.inverse_ref, ...), custom_call_target="tpu_custom_call" | custom-call | tf_op jit(solution)/shard_map/sparse_attention/pallas_call | solution.py:395
  42.8 1.8 %copy.8 = bf16[384,512]{1,0:T(8,128)(2,1)} copy(bf16[384,512]{1,0:T(8,128)(2,1)} %sparse_attention.1) | data formatting | bytes 786432
  (1 shorter events, 0.0 us)
